TPU v7x, 32 devices: a whole 2x2x4 slice. The times are simulated.
32 devices in a mesh: fs: 8 (over z, y), tp: 4 (over x, core).
Axes of the slice: x: 2, y: 2, z: 4, core: 2. Of those that a mesh axis runs over, the one named last changes fastest.
Arguments:
- late_input: bfloat16 [2048, 2048], P(('fs', 'tp')), may hold values from -6 to 6
- early_input: bfloat16 [2048, 2048], P(('fs', 'tp')), may hold values from -6 to 6
- early_grad: bfloat16 [2048, 2048], P(('fs', 'tp')), may hold values from -6 to 6
- pre_gain: float32 [2048], replicated, may hold values from 0.1 to 1.9
- post_gain: float32 [2048], replicated, may hold values from 0.1 to 1.9
- gate_weight: bfloat16 [2048, 4096], P('fs', 'tp'), may hold values from -0.125 to 0.125
- up_weight: bfloat16 [2048, 4096], P('fs', 'tp'), may hold values from -0.125 to 0.125
- down_weight: bfloat16 [2048, 4096], P('fs', 'tp'), may hold values from -0.09375 to 0.09375
- gate_sum: float32 [2048, 4096], P('fs', 'tp'), may hold values from -1.8 to 1.8
- up_sum: float32 [2048, 4096], P('fs', 'tp'), may hold values from -1.8 to 1.8
- down_gradient_sum: float32 [2048, 4096], P('fs', 'tp'), may hold values from -1.8 to 1.8
Outputs:
- late_output: bfloat16 [2048, 2048], P(('fs', 'tp'))
- early_input_grad: bfloat16 [2048, 2048], P(('fs', 'tp'))
- gate_total: float32 [2048, 4096], P('fs', 'tp')
- up_total: float32 [2048, 4096], P('fs', 'tp')
- down_total: float32 [2048, 4096], P('fs', 'tp')
All inputs are finite; a program needn't handle non-finite values.
Results may differ from a plain program's by a relative error of at most 0.013.
Values may be sent and summed in bfloat16 or wider, within the bound.
A program may use at most 128 MiB of HBM per device.

v0:
```python
import functools
import math

import jax
import jax.numpy as jnp
from jax import lax
from jax.experimental import pallas as pl
from jax.experimental.pallas import tpu as pltpu
from jax.sharding import PartitionSpec as P

NORM_EPS = 1e-06
PAIR = 2
MESH = pl.DeviceIdType.MESH
VMEM_LIMIT = 60 * 1024 * 1024


def contract_last(first_op, second_op):
    return lax.dot_general(
        first_op, second_op, (((1,), (1,)), ((), ())), preferred_element_type=jnp.float32
    )


def contract_first(first_op, second_op):
    return lax.dot_general(
        first_op, second_op, (((0,), (0,)), ((), ())), preferred_element_type=jnp.float32
    )


def inverse_rms(values):
    return lax.rsqrt(jnp.mean(values * values, axis=-1, keepdims=True) + NORM_EPS)


class Place:
    def __init__(self, n_fs, n_tp):
        self.line_len, self.n_tp = n_fs // PAIR, n_tp
        self.group = PAIR * n_tp
        self.fs, self.tp = lax.axis_index("fs"), lax.axis_index("tp")
        self.line, self.side = self.fs // PAIR, self.fs % PAIR
        self.member = self.side * n_tp + self.tp
        self.core = self.tp % PAIR
        self.chip = self.member // PAIR
        self.up = {"fs": self.fs + PAIR, "tp": self.tp}
        self.down = {"fs": self.fs - PAIR, "tp": self.tp}
        self.across = {"fs": self.line * PAIR + 1 - self.side, "tp": self.tp}
        self.has_up, self.has_down = self.line < self.line_len - 1, self.line > 0

    def member_id(self, member):
        return {"fs": self.line * PAIR + member // self.n_tp, "tp": member % self.n_tp}

    def enter(self, on_line):
        barrier = pltpu.get_barrier_semaphore()

        def greet(who):
            pl.semaphore_signal(barrier, inc=1, device_id=who, device_id_type=MESH)

        for offset in range(1, self.group):
            greet(self.member_id((self.member + offset) % self.group))
        if on_line:
            pl.when(self.has_up)(lambda: greet(self.up))
            pl.when(self.has_down)(lambda: greet(self.down))
        peers = self.group - 1
        if on_line:
            peers += self.has_up.astype(jnp.int32) + self.has_down.astype(jnp.int32)
        pl.semaphore_wait(barrier, peers)


def remote(src, dst, send_sem, recv_sem, who):
    return pltpu.make_async_remote_copy(
        src_ref=src,
        dst_ref=dst,
        send_sem=send_sem,
        recv_sem=recv_sem,
        device_id=who,
        device_id_type=MESH,
    )


def gather_kernel(
    n_fs,
    n_tp,
    late_ref,
    early_ref,
    gain_ref,
    *refs,
):
    w_refs, (late_out, early_out), w_outs = refs[:3], refs[3:5], refs[5:8]
    gate_out, up_out, hidden_out, normed = refs[8:12]
    tok_send, tok_recv, own_sem, across_send, up_send, down_send, w_recv = refs[12:]
    at = Place(n_fs, n_tp)
    half = w_outs[0].shape[2]
    kept = pl.ds(pl.multiple_of(at.side * half, half), half)
    given = pl.ds(pl.multiple_of((1 - at.side) * half, half), half)
    at.enter(True)

    def slot_of(line, turn):
        return line * PAIR + (at.side if turn == 0 else 1 - at.side)

    def carry(w, slot, src, send_sem, who):
        return remote(src, w_outs[w].at[slot], send_sem, w_recv.at[w, slot], who)

    across, own, tokens = [], [], []
    for w in range(3):
        across.append(
            carry(w, at.fs, w_refs[w].at[:, given], across_send.at[w], at.across)
        )
        across[-1].start()
    flows = []
    for step in range(at.line_len):
        for w in range(3):
            for turn in range(PAIR):
                from_low, from_high = at.line - step, at.line + step
                low = jnp.maximum(from_low, 0)
                high = jnp.minimum(from_high, at.line_len - 1)
                flows.append((step, w, turn, from_low >= 0, from_high < at.line_len, low, high))

    def flow_copies(flow):
        step, w, turn, _, _, low, high = flow
        own_block = step == 0 and turn == 0
        copies = []
        for line, sems, who in ((low, up_send, at.up), (high, down_send, at.down)):
            slot = slot_of(line, turn)
            src = w_refs[w].at[:, kept] if own_block else w_outs[w].at[slot]
            copies.append(carry(w, slot, src, sems.at[w, step, turn], who))
        return copies

    def run(flow):
        step, w, turn, low_ok, high_ok, _, _ = flow
        up_copy, down_copy = flow_copies(flow)
        if step == 0 and turn == 1:
            up_copy.wait_recv()
        if step > 0:
            pl.when(low_ok)(up_copy.wait_recv)
        pl.when(low_ok & at.has_up)(up_copy.start)
        if step > 0:
            pl.when(high_ok)(down_copy.wait_recv)
        pl.when(high_ok & at.has_down)(down_copy.start)

    def run_where(weights, turns, forwarded):
        for flow in flows:
            if flow[1] in weights and flow[2] in turns and (flow[0] > 0) == forwarded:
                run(flow)

    run_where((0, 1), (0,), False)
    for w in range(3):
        own.append(
            pltpu.make_async_copy(w_refs[w].at[:, kept], w_outs[w].at[at.fs], own_sem.at[w])
        )
        own[-1].start()
    for part, (src, dst) in enumerate(((late_ref, late_out), (early_ref, early_out))):
        values = src[...].astype(jnp.float32)
        normed[part] = (values * inverse_rms(values) * gain_ref[...]).astype(jnp.bfloat16)
        dst[at.member] = normed[part]
    run_where((0, 1), (1,), False)
    for part, dst in ((1, early_out), (0, late_out)):
        for offset in range(1, at.group):
            copy = remote(
                normed.at[part],
                dst.at[at.member],
                tok_send.at[part, offset],
                tok_recv.at[part, offset],
                at.member_id((at.member + offset) % at.group),
            )
            copy.start()
            tokens.append(copy)
    run_where((0,), (0, 1), True)
    run_where((2,), (0, 1), False)
    run_where((1,), (0, 1), True)
    for copy in own:
        copy.wait()
    for copy in tokens[: at.group - 1]:
        copy.wait_recv()
    owners = min(at.group, 4)
    tile = owners * early_ref.shape[0]

    @pl.loop(0, at.group // owners)
    def _(i):
        span = pl.ds(pl.multiple_of(i * tile, tile), tile)
        rows = early_out[pl.ds(i * owners, owners)].reshape(tile, early_ref.shape[1])

        def product(w):
            return jnp.dot(
                rows, w_outs[w][...].reshape(-1, half), preferred_element_type=jnp.float32
            )

        gate, up = product(0), product(1)
        gate_out[span] = gate
        up_out[span] = up
        hidden_out[span] = (gate * jax.nn.sigmoid(gate) * up).astype(jnp.bfloat16)

    run_where((2,), (0, 1), True)
    for copy in tokens[at.group - 1 :]:
        copy.wait_recv()
    for copy in tokens:
        copy.wait_send()
    for copy in across:
        copy.wait_send()
    for flow in flows:
        up_copy, down_copy = flow_copies(flow)
        pl.when(flow[3] & at.has_up)(up_copy.wait_send)
        pl.when(flow[4] & at.has_down)(down_copy.wait_send)


def mixed_kernel(
    n_fs,
    n_tp,
    part_ref,
    grad_ref,
    gain_ref,
    out_ref,
    pair_in,
    pair_sum,
    sums_in,
    total,
    cot,
    pair_send,
    pair_recv,
    sum_send,
    sum_recv,
    cot_send,
    cot_recv,
    relay_send,
    relay_recv,
):
    at = Place(n_fs, n_tp)
    chips = at.group // PAIR
    partner = at.member_id(at.member + 1 - 2 * at.core)
    at.enter(False)

    def chip_at(offset):
        return (at.chip + offset) % chips

    def member_at(offset):
        return chip_at(offset) * PAIR + at.core

    order = list(range(1, chips)) + [0]
    halves = {}
    for offset in order:
        theirs = chip_at(offset) * PAIR + 1 - at.core
        halves[offset] = remote(
            part_ref.at[theirs],
            pair_in.at[offset],
            pair_send.at[offset],
            pair_recv.at[offset],
            partner,
        )
        halves[offset].start()
    sums = []
    for offset in order:
        halves[offset].wait_recv()
        both = part_ref[member_at(offset)].astype(jnp.float32) + pair_in[offset].astype(jnp.float32)
        if offset == 0:
            total[...] = both
            continue
        pair_sum[offset] = both.astype(jnp.bfloat16)
        copy = remote(
            pair_sum.at[offset],
            sums_in.at[offset],
            sum_send.at[offset],
            sum_recv.at[offset],
            at.member_id(member_at(offset)),
        )
        copy.start()
        sums.append(copy)
    for offset, copy in zip(order, sums):
        copy.wait_recv()
        total[...] += sums_in[offset].astype(jnp.float32)
    mixed = total[...].astype(jnp.bfloat16).astype(jnp.float32)
    inverse = inverse_rms(mixed)
    weighted = 0.5 * grad_ref[...].astype(jnp.float32) * gain_ref[...]
    cot[...] = (
        inverse * weighted
        - mixed * inverse**3 * jnp.mean(weighted * mixed, axis=-1, keepdims=True)
    ).astype(jnp.bfloat16)
    sends = []
    for offset in order:
        who = partner if offset == 0 else at.member_id(member_at(offset))
        sends.append(
            remote(cot, out_ref.at[at.member], cot_send.at[offset], cot_recv.at[offset], who)
        )
        sends[-1].start()
    out_ref[at.member] = cot[...]
    relays = []
    for offset, copy in zip(order, sends):
        copy.wait_recv()
        if offset == 0:
            continue
        slot = member_at(chips - offset)
        relay = remote(
            out_ref.at[slot], out_ref.at[slot], relay_send.at[offset], relay_recv.at[offset], partner
        )
        relay.start()
        relays.append(relay)
    for relay in relays:
        relay.wait()
    for copy in list(halves.values()) + sums + sends:
        copy.wait_send()


def scatter_kernel(n_fs, n_tp, grad_scale, *refs):
    cot_ref, hidden_ref = refs[:2]
    outs, tok_outs = refs[9:12], refs[12:14]
    staged = refs[14:21]
    early_ref, down_ref, gate_ref, up_ref, gate_w, up_w, late_ref = staged
    parts, below, above, given, total, gate_cot, up_cot, tok_parts, tok_in = refs[21:30]
    (
        stage_sem,
        tok_send,
        tok_recv,
        up_send,
        up_recv,
        down_send,
        down_recv,
        across_send,
        across_recv,
    ) = refs[30:]
    at = Place(n_fs, n_tp)
    rows, tok_rows = parts.shape[2], tok_parts.shape[2]
    piece = min(rows, 64)
    owners = min(at.group, 4)
    tile = owners * tok_rows
    loads = [
        pltpu.make_async_copy(src, dst, stage_sem.at[i])
        for i, (src, dst) in enumerate(zip(refs[2:9], staged))
    ]
    for load in loads:
        load.start()
    at.enter(True)

    def over_rows(body):
        @pl.loop(0, rows // piece)
        def _(i):
            body(pl.ds(pl.multiple_of(i * piece, piece), piece))

    def over_tokens(body):
        @pl.loop(0, at.group // owners)
        def _(i):
            body(pl.ds(pl.multiple_of(i * tile, tile), tile), pl.ds(i * owners, owners))

    def grad_part(w, left_ref, right_ref):
        @pl.loop(0, n_fs)
        def _(slot):
            left = left_ref[:, pl.ds(pl.multiple_of(slot * rows, rows), rows)]
            parts[w, slot] = (grad_scale * contract_first(left, right_ref[...])).astype(
                jnp.bfloat16
            )

    def slots_of(w):
        for step in range(at.line_len - 1):
            for turn in range(PAIR):
                side = 1 - at.side if turn == 0 else at.side
                top, bottom = at.line_len - 1 - step, step
                yield top, top * PAIR + side, bottom, bottom * PAIR + side

    def hop(w, slot, src, upward):
        held, send, recv, who = (
            (below, up_send, up_recv, at.up) if upward else (above, down_send, down_recv, at.down)
        )
        src = held.at[w, slot] if src is None else src
        return remote(src, held.at[w, slot], send.at[w, slot], recv.at[w, slot], who)

    def first_sends(w):
        @pl.when(at.line == 0)
        def _():
            for _, slot, _, _ in slots_of(w):
                hop(w, slot, parts.at[w, slot], True).start()

        @pl.when(at.line == at.line_len - 1)
        def _():
            for _, _, _, slot in slots_of(w):
                hop(w, slot, parts.at[w, slot], False).start()

    def pass_on(w, slot, upward):
        copy = hop(w, slot, None, upward)
        held = below if upward else above
        copy.wait_recv()

        def add(span):
            held[w, slot, span] = (
                held[w, slot, span].astype(jnp.float32) + parts[w, slot, span].astype(jnp.float32)
            ).astype(jnp.bfloat16)

        over_rows(add)
        copy.start()

    def middle_sends(w):
        for top, up_slot, bottom, down_slot in slots_of(w):
            pl.when((at.line > 0) & (at.line < top))(
                functools.partial(pass_on, w, up_slot, True)
            )
            pl.when((at.line < at.line_len - 1) & (at.line > bottom))(
                functools.partial(pass_on, w, down_slot, False)
            )

    tokens = [[], []]

    def send_tokens(which):
        for offset in range(1, at.group):
            member = (at.member + offset) % at.group
            copy = remote(
                tok_parts.at[which, member],
                tok_in.at[which, offset],
                tok_send.at[which, offset],
                tok_recv.at[which, offset],
                at.member_id(member),
            )
            copy.start()
            tokens[which].append(copy)

    def by_owner(product):
        return product.astype(jnp.bfloat16).reshape(owners, tok_rows, product.shape[-1])

    def cots(span, _):
        hidden_cot = jnp.dot(cot_ref[span], down_ref[...], preferred_element_type=jnp.float32)
        gate, up = gate_ref[span], up_ref[span]
        sigmoid = jax.nn.sigmoid(gate)
        gate_cot[span] = (hidden_cot * up * sigmoid * (1.0 + gate * (1.0 - sigmoid))).astype(
            jnp.bfloat16
        )
        up_cot[span] = (hidden_cot * gate * sigmoid).astype(jnp.bfloat16)

    def normed_part(span, owned):
        tok_parts[0, owned] = by_owner(
            contract_last(gate_cot[span], gate_w[...]) + contract_last(up_cot[span], up_w[...])
        )

    def late_part(span, owned):
        late = late_ref[span]
        gate = jnp.dot(late, gate_w[...], preferred_element_type=jnp.float32)
        up = jnp.dot(late, up_w[...], preferred_element_type=jnp.float32)
        hidden = (gate * jax.nn.sigmoid(gate) * up).astype(jnp.bfloat16)
        tok_parts[1, owned] = by_owner(contract_last(hidden, down_ref[...]))

    across = []

    def finish(w):
        for turn in range(PAIR):
            side = 1 - at.side if turn == 0 else at.side
            slot = at.line * PAIR + side

            def first(span):
                total[span] = parts[w, slot, span].astype(jnp.float32)

            def arrive(upward):
                held = below if upward else above
                hop(w, slot, None, upward).wait_recv()

                def add(span):
                    total[span] += held[w, slot, span].astype(jnp.float32)

                over_rows(add)

            over_rows(first)
            pl.when(at.has_down)(functools.partial(arrive, True))
            pl.when(at.has_up)(functools.partial(arrive, False))
            if turn == 0:

                def give(span):
                    given[w, span] = total[span].astype(jnp.bfloat16)

                over_rows(give)
                copy = remote(
                    given.at[w], outs[w].at[at.side], across_send.at[w], across_recv.at[w], at.across
                )
                copy.start()
                across.append(copy)
            else:

                def keep(span):
                    outs[w][at.side, span] = total[span].astype(jnp.bfloat16)

                over_rows(keep)

    grad_part(2, cot_ref, hidden_ref)
    first_sends(2)
    for load in loads[:4]:
        load.wait()
    over_tokens(cots)
    grad_part(0, early_ref, gate_cot)
    first_sends(0)
    grad_part(1, early_ref, up_cot)
    first_sends(1)
    for load in loads[4:]:
        load.wait()
    over_tokens(normed_part)
    send_tokens(0)
    middle_sends(2)
    over_tokens(late_part)
    send_tokens(1)
    middle_sends(0)
    finish(2)
    for which in range(2):
        running = tok_parts[which, at.member].astype(jnp.float32)
        for offset, copy in enumerate(tokens[which], 1):
            copy.wait_recv()
            running = running + tok_in[which, offset].astype(jnp.float32)
        tok_outs[which][...] = running.astype(jnp.bfloat16)
        if which == 0:
            middle_sends(1)
            finish(0)
    finish(1)
    for copy in across:
        copy.wait()
    for copy in tokens[0] + tokens[1]:
        copy.wait_send()
    for w in range(3):
        for top, up_slot, bottom, down_slot in slots_of(w):
            pl.when(at.line < top)(hop(w, up_slot, None, True).wait_send)
            pl.when(at.line > bottom)(hop(w, down_slot, None, False).wait_send)


def call(kernel, collective_id, operands, out_shapes, scratch, flops, n_any=0):
    in_vmem = pl.BlockSpec(memory_space=pltpu.VMEM)
    in_any = pl.BlockSpec(memory_space=pl.ANY)
    return pl.pallas_call(
        kernel,
        out_shape=out_shapes,
        in_specs=[in_vmem] * (len(operands) - n_any) + [in_any] * n_any,
        out_specs=[in_vmem] * len(out_shapes),
        scratch_shapes=scratch,
        cost_estimate=pl.CostEstimate(flops=flops, bytes_accessed=0, transcendentals=0),
        compiler_params=pltpu.CompilerParams(
            collective_id=collective_id, has_side_effects=True, vmem_limit_bytes=VMEM_LIMIT
        ),
    )(*operands)


def per_device(
    n_fs,
    n_tp,
    late_input,
    early_input,
    early_grad,
    pre_gain,
    post_gain,
    gate_weight,
    up_weight,
    down_weight,
    gate_sum,
    up_sum,
    down_gradient_sum,
):
    tok_rows, model_width = late_input.shape
    shard_rows, hidden_width = gate_weight.shape
    half = hidden_width // PAIR
    group = PAIR * n_tp
    chips = group // PAIR
    line_len = n_fs // PAIR
    group_rows = group * tok_rows
    grad_scale = 1.0 / math.sqrt(tok_rows * n_tp * n_fs)
    dma = pltpu.SemaphoreType.DMA
    bf16 = jnp.bfloat16

    def shaped(*shape):
        return jax.ShapeDtypeStruct(shape, bf16)

    late_values = late_input.astype(jnp.float32)
    early_values = early_input.astype(jnp.float32)
    early_in_inverse = inverse_rms(early_values)
    preact = jax.ShapeDtypeStruct((group_rows, half), jnp.float32)
    tok_block = shaped(group, tok_rows, model_width)
    w_block = shaped(n_fs, shard_rows, half)
    late_rows, early_rows, gate_all, up_all, down_all, early_gate, early_up, early_hidden = call(
        functools.partial(gather_kernel, n_fs, n_tp),
        0,
        (
            late_input,
            early_input,
            pre_gain.reshape(1, model_width),
            gate_weight,
            up_weight,
            down_weight,
        ),
        [tok_block] * 2 + [w_block] * 3 + [preact, preact, shaped(group_rows, half)],
        [
            pltpu.VMEM((2, tok_rows, model_width), bf16),
            dma((2, group)),
            dma((2, group)),
            dma((3,)),
            dma((3,)),
            dma((3, line_len, PAIR)),
            dma((3, line_len, PAIR)),
            dma((3, n_fs)),
        ],
        10**9,
    )
    late_rows = late_rows.reshape(group_rows, model_width)
    early_rows = early_rows.reshape(group_rows, model_width)
    gate_all, up_all, down_all = (
        full.reshape(model_width, half) for full in (gate_all, up_all, down_all)
    )

    def by_owner(product):
        return product.astype(bf16).reshape(group, tok_rows, model_width)

    early_part = by_owner(contract_last(early_hidden, down_all))
    chip_block = pltpu.VMEM((chips, tok_rows, model_width), bf16)
    (cot_rows,) = call(
        functools.partial(mixed_kernel, n_fs, n_tp),
        1,
        (early_part, early_grad, post_gain.reshape(1, model_width)),
        [tok_block],
        [
            chip_block,
            chip_block,
            chip_block,
            pltpu.VMEM((tok_rows, model_width), jnp.float32),
            pltpu.VMEM((tok_rows, model_width), bf16),
        ]
        + [dma((chips,))] * 8,
        10**8,
    )
    cot_rows = cot_rows.reshape(group_rows, model_width)
    staged = (early_rows, down_all, early_gate, early_up, gate_all, up_all, late_rows)
    own_tokens = shaped(tok_rows, model_width)
    own_shard = shaped(PAIR, shard_rows, half)
    line_block = pltpu.VMEM((3, n_fs, shard_rows, half), bf16)
    *grads, normed_cot, late_mixed = call(
        functools.partial(scatter_kernel, n_fs, n_tp, grad_scale),
        2,
        (cot_rows, early_hidden, *staged),
        [own_shard, own_shard, own_shard, own_tokens, own_tokens],
        [pltpu.VMEM(array.shape, array.dtype) for array in staged]
        + [
            line_block,
            line_block,
            line_block,
            pltpu.VMEM((3, shard_rows, half), bf16),
            pltpu.VMEM((shard_rows, half), jnp.float32),
            pltpu.VMEM((group_rows, half), bf16),
            pltpu.VMEM((group_rows, half), bf16),
            pltpu.VMEM((2, group, tok_rows, model_width), bf16),
            pltpu.VMEM((2, group, tok_rows, model_width), bf16),
            dma((len(staged),)),
            dma((2, group)),
            dma((2, group)),
        ]
        + [dma((3, n_fs))] * 4
        + [dma((3,))] * 2,
        10**9,
        n_any=len(staged),
    )
    late_mixed = late_mixed.astype(jnp.float32)
    late_output = (
        late_values + 0.5 * late_mixed * inverse_rms(late_mixed) * post_gain
    ).astype(bf16)
    weighted_in = normed_cot.astype(jnp.float32) * pre_gain
    early_input_grad = (
        early_grad.astype(jnp.float32)
        + early_in_inverse * weighted_in
        - early_values
        * early_in_inverse**3
        * jnp.mean(weighted_in * early_values, axis=-1, keepdims=True)
    ).astype(bf16)
    totals = [
        running + jnp.concatenate([grad[0], grad[1]], axis=1).astype(jnp.float32)
        for running, grad in zip((gate_sum, up_sum, down_gradient_sum), grads)
    ]
    return (late_output, early_input_grad, *totals)


def solution(mesh):
    in_specs = (
        P(("fs", "tp"), None),
        P(("fs", "tp"), None),
        P(("fs", "tp"), None),
        P(),
        P(),
        P("fs", "tp"),
        P("fs", "tp"),
        P("fs", "tp"),
        P("fs", "tp"),
        P("fs", "tp"),
        P("fs", "tp"),
    )
    out_specs = (
        P(("fs", "tp"), None),
        P(("fs", "tp"), None),
        P("fs", "tp"),
        P("fs", "tp"),
        P("fs", "tp"),
    )
    return jax.shard_map(
        functools.partial(per_device, mesh.shape["fs"], mesh.shape["tp"]),
        mesh=mesh, in_specs=in_specs, out_specs=out_specs, check_vma=False
    )
```

profile of v0, /device:TPU:0, one launch (start us, length us, event | category | flops | bytes accessed | tf_op | source)
XLA Modules:
  0.0 282.8 jit_solution(5110987114725073914)
XLA Ops:
  0.6 114.9 %shard_map.146 = (bf16[8,64,2048]{2,1,0:T(8,128)(2,1)}, bf16[8,64,2048]{2,1,0:T(8,128)(2,1)}, bf16[8,256,512]{2,1,0:T(8,128)(2,1)}, bf16[8,256,512]{2,1,0:T(8,12...) custom-call(bf16[64,2048]{1,0:T(8,128)(2,1)} %late_ref.1, ...), custom_call_target="tpu_custom_call" | custom-call | flops 1000000000 | tf_op jit(solution)/shard_map/pallas_call | solution.py:514
  115.6 4.4 %convolution_convert_fusion = bf16[512,2048]{1,0:T(8,128)(2,1)} fusion(bf16[512,512]{1,0:T(8,128)(2,1)} %get-tuple-element.18.refs_1_, bf16[2048,512]{1,0:T(8,128)(2,1)} %bitcast.29), kind=kOutput, calls=%fused_computation | convolution fusion | flops 1074790400 | bytes 4718592 | tf_op jit(solution)/shard_map/dot_general | solution.py:18
  120.0 34.4 %shard_map.147 = bf16[8,64,2048]{2,1,0:T(8,128)(2,1)} custom-call(bf16[8,64,2048]{2,1,0:T(8,128)(2,1)} %bitcast.24, bf16[64,2048]{1,0:T(8,128)(2,1)} %grad_ref.1, f32[1,2048]{1,0:T(1,128)} %bitcast.31), custom_call_target="tpu_custom_call" | custom-call | flops 100000000 | tf_op jit(solution)/shard_map/pallas_call | solution.py:514
  154.3 0.0 copy-start.1
  154.3 0.0 copy-start.10
  154.3 0.0 copy-start.8
  154.4 0.0 copy-start.9
  154.4 119.1 %shard_map.148 = (bf16[2,256,512]{2,1,0:T(8,128)(2,1)}, bf16[2,256,512]{2,1,0:T(8,128)(2,1)}, bf16[2,256,512]{2,1,0:T(8,128)(2,1)}, bf16[64,2048]{1,0:T(8,128)(2,1)}, bf16[64,2048]{1,0:T(8,128)(2,1)}) custom-call(bf16[512,2048]{1,0:T(8,128)(2,1)} %bitcast.23, bf16[512,512]{1,0:T(8,128)(2,1)} %get-tuple-element.18.refs_1_, bf16[512,2048]{1,0:T(8,128)(2,1)} %bitcast.26, ...), custom_call_target="tpu_custom_call" | custom-call | flops 1000000000 | tf_op jit(solution)/shard_map/pallas_call | solution.py:514
  273.5 0.0 copy-start
  273.5 0.0 copy-start.3
  273.5 1.2 slice_bitcast_fusion.5
  274.7 1.3 fusion.4
  276.1 0.0 copy-done.8
  276.1 0.0 copy-done.9
  276.1 0.0 copy-start.6
  276.1 0.0 copy-start.7
  276.1 1.9 fusion.3
  278.0 1.0 fusion.7
  279.0 0.0 copy-done.3
  279.0 1.1 convert_add_fusion.2
  280.1 0.1 slice_bitcast_fusion.1
  280.2 0.4 copy-done.4
  280.6 1.1 convert_add_fusion
  281.7 1.1 convert_add_fusion.1
  (13 shorter events, 0.0 us)
Async XLA Ops:
  154.3 120.4 %copy-start.1 = (bf16[64,2048]{1,0:T(8,128)(2,1)S(1)}, bf16[64,2048]{1,0:T(8,128)(2,1)}, u32[]{:S(2)}) copy-start(bf16[64,2048]{1,0:T(8,128)(2,1)} %early_ref.1) | copy-start | bytes 786436
  154.3 120.3 %copy-start.10 = (f32[2048]{0:T(1024)S(1)}, f32[2048]{0:T(1024)}, u32[]{:S(2)}) copy-start(f32[2048]{0:T(1024)} %param.14) | copy-start | bytes 24580
  154.3 121.7 %copy-start.8 = (bf16[64,2048]{1,0:T(8,128)(2,1)S(1)}, bf16[64,2048]{1,0:T(8,128)(2,1)}, u32[]{:S(2)}) copy-start(bf16[64,2048]{1,0:T(8,128)(2,1)} %late_ref.1) | copy-start | bytes 786436
  154.4 121.7 %copy-start.9 = (f32[2048]{0:T(1024)S(1)}, f32[2048]{0:T(1024)}, u32[]{:S(2)}) copy-start(f32[2048]{0:T(1024)} %param.15) | copy-start | bytes 24580
  273.5 4.6 %copy-start = (bf16[64,2048]{1,0:T(8,128)(2,1)S(1)}, bf16[64,2048]{1,0:T(8,128)(2,1)}, u32[]{:S(2)}) copy-start(bf16[64,2048]{1,0:T(8,128)(2,1)} %grad_ref.1) | copy-start | bytes 786436
  273.5 4.5 %copy-start.2 = (bf16[64,2048]{1,0:T(8,128)(2,1)S(1)}, bf16[64,2048]{1,0:T(8,128)(2,1)}, u32[]{:S(2)}) copy-start(bf16[64,2048]{1,0:T(8,128)(2,1)} %get-tuple-element.27) | copy-start | bytes 786436
  273.5 5.5 %copy-start.3 = (f32[256,1024]{1,0:T(8,128)S(1)}, f32[256,1024]{1,0:T(8,128)}, u32[]{:S(2)}) copy-start(f32[256,1024]{1,0:T(8,128)} %param.19) | copy-start | bytes 3145732
  276.1 4.0 %copy-start.6 = (bf16[2,256,512]{2,1,0:T(8,128)(2,1)S(1)}, bf16[2,256,512]{2,1,0:T(8,128)(2,1)}, u32[]{:S(2)}) copy-start(bf16[2,256,512]{2,1,0:T(8,128)(2,1)} %get-tuple-element.29) | copy-start | bytes 1572868
  276.1 4.0 %copy-start.7 = (bf16[2,256,512]{2,1,0:T(8,128)(2,1)S(1)}, bf16[2,256,512]{2,1,0:T(8,128)(2,1)}, u32[]{:S(2)}) copy-start(bf16[2,256,512]{2,1,0:T(8,128)(2,1)} %get-tuple-element.30) | copy-start | bytes 1572868
  279.0 1.6 copy-start.4
  280.1 1.6 copy-start.5
where the time goes:
time: 286 us; the launch traced here: 283 us
  Pallas kernels  268 us (94%)
  other arithmetic  7.56 us (3%)
  matrix products  4.38 us (2%)
    pallas_call x3, Pallas kernels, call(): pl.pallas_call(kernel, out_shape=out_shapes, in_specs=[in_vmem] * (len(op...  268 us

commit v1 on v0

v1 whole, which is shorter than its diff:
```python
import functools
import math

import jax
import jax.numpy as jnp
from jax import lax
from jax.experimental import pallas as pl
from jax.experimental.pallas import tpu as pltpu
from jax.sharding import PartitionSpec as P

NORM_EPS = 1e-06
PAIR = 2
GROUP = 16
LATE, EARLY = 0, 1
GATE, UP, DOWN = 0, 1, 2
MESH = pl.DeviceIdType.MESH
VMEM_LIMIT = 60 * 1024 * 1024
BF16, F32 = jnp.bfloat16, jnp.float32


def contract_last(first_op, second_op):
    return lax.dot_general(
        first_op, second_op, (((1,), (1,)), ((), ())), preferred_element_type=F32
    )


def contract_first(first_op, second_op):
    return lax.dot_general(
        first_op, second_op, (((0,), (0,)), ((), ())), preferred_element_type=F32
    )


def inverse_rms(values):
    return lax.rsqrt(jnp.mean(values * values, axis=-1, keepdims=True) + NORM_EPS)


def quad_of(n_fs, n_tp):
    return min(n_fs, max(1, GROUP // n_tp))


class Place:
    def __init__(self, n_fs, n_tp):
        self.n_fs, self.n_tp = n_fs, n_tp
        self.quad = quad_of(n_fs, n_tp)
        self.groups, self.xs = n_fs // self.quad, n_tp // PAIR
        self.fs, self.tp = lax.axis_index("fs"), lax.axis_index("tp")
        self.g, self.q = self.fs // self.quad, self.fs % self.quad
        self.x, self.core = self.tp // PAIR, self.tp % PAIR
        self.me = self.member(0, 0, self.core)
        self.partner = self.device(0, 0, 1 - self.core)

    def at_q(self, dq):
        return (self.q + self.quad + dq) % self.quad

    def at_x(self, dx):
        return (self.x + self.xs + dx) % self.xs

    def at_g(self, dg):
        return (self.g + dg) % self.groups

    def member(self, dq, dx, core):
        return self.at_q(dq) * self.n_tp + self.at_x(dx) * PAIR + core

    def device(self, dq, dx, core):
        return {"fs": self.g * self.quad + self.at_q(dq), "tp": self.at_x(dx) * PAIR + core}

    def slot(self, dg, dq):
        return self.at_g(dg) * self.quad + self.at_q(dq)

    def enter(self):
        barrier = pltpu.get_barrier_semaphore()

        def greet(fs, tp):
            pl.semaphore_signal(
                barrier, inc=1, device_id={"fs": fs, "tp": tp}, device_id_type=MESH
            )

        peers = 0
        for offset in range(1, self.n_fs):
            greet((self.fs + offset) % self.n_fs, self.tp)
            peers += 1
        for dq in range(self.quad):
            for offset in range(1, self.n_tp):
                greet(self.g * self.quad + self.at_q(dq), (self.tp + offset) % self.n_tp)
                peers += 1
        pl.semaphore_wait(barrier, peers)


def remote(src, dst, send_sem, recv_sem, who):
    return pltpu.make_async_remote_copy(
        src_ref=src,
        dst_ref=dst,
        send_sem=send_sem,
        recv_sem=recv_sem,
        device_id=who,
        device_id_type=MESH,
    )


def layer_kernel(n_fs, n_tp, grad_scale, *refs):
    late_ref, early_ref, grad_ref, pre_ref, post_ref = refs[:5]
    w_refs = refs[5:8]
    late_out, early_out = refs[8:10]
    grad_outs = refs[10:13]
    normed, weights, gate, up, hidden, cots, parts, pair_in, sums_in, total = refs[13:23]
    gate_cot, up_cot, grad_parts, grad_in = refs[23:27]
    w_send, w_recv, g_send, g_recv, sems = refs[27:]

    at = Place(n_fs, n_tp)
    quad, xs, groups = at.quad, at.xs, at.groups
    tok_rows, width = early_ref.shape
    rows, units = weights.shape[2:]
    tile = n_tp * tok_rows
    everything = pl.ds(0, width)
    chunk = quad * rows
    offsets = [(dq, dx) for dq in range(quad) for dx in range(xs)]
    others = offsets[1:]
    pending = []

    def start(copy):
        copy.start()
        pending.append(copy)

    def w_copy(w, dg, dq):
        source = w_refs[w].at[:, pl.ds(pl.multiple_of(at.at_q(dq) * units, units), units)]
        who = {"fs": at.slot(dg, dq), "tp": at.tp}
        return remote(
            source, weights.at[w, at.fs], w_send.at[w, dg, dq], w_recv.at[w, dg, dq], who
        )

    q_order = [2, 1, 3, 0] if quad == 4 else list(range(quad - 1, -1, -1))

    def send_weights(w):
        for dq in q_order:
            for dg in range(groups - 1, -1, -1):
                if dg or dq:
                    start(w_copy(w, dg, dq))

    def wait_weights(w, dgs):
        for dg in dgs:
            for dq in q_order:
                if dg or dq:
                    w_copy(w, dg, dq).wait_recv()

    def all_rows(w):
        return weights[w].reshape(n_fs * rows, units)

    def ici(inst, dq, dx, src, dst, who):
        return remote(src, dst, sems.at[inst, 0, dq, dx], sems.at[inst, 1, dq, dx], who)

    def pair(inst, dq, dx, src, dst):
        return remote(src, dst, sems.at[inst, 2, dq, dx], sems.at[inst, 3, dq, dx], at.partner)

    def gather_copy(inst, buf, dq, dx, direct):
        if direct or dx == 0:
            block = buf.at[at.me]
            return ici(inst, dq, dx, block, block, at.device(dq, dx, at.core))
        block = buf.at[at.member(-dq, 0, at.core)]
        return ici(inst, dq, dx, block, block, at.device(0, dx, at.core))

    def gather_pair(inst, buf, dq, dx):
        block = buf.at[at.member(-dq, -dx, at.core)]
        return pair(inst, dq, dx, block, block)

    def gather_start(inst, buf, direct):
        for dq, dx in others:
            if direct or dq == 0 or dx == 0:
                start(gather_copy(inst, buf, dq, dx, direct))
        start(gather_pair(inst, buf, 0, 0))

    def gather_pass_on(inst, buf, direct):
        if not direct:
            for dq in range(1, quad):
                gather_copy(inst, buf, dq, 0, direct).wait_recv()
                for dx in range(1, xs):
                    start(gather_copy(inst, buf, dq, dx, direct))
                start(gather_pair(inst, buf, dq, 0))
        for dq, dx in others:
            if direct or dx:
                gather_copy(inst, buf, dq, dx, direct).wait_recv()
                start(gather_pair(inst, buf, dq, dx))

    def gather_wait(inst, buf):
        for dq, dx in offsets:
            gather_pair(inst, buf, dq, dx).wait_recv()

    def sum_pair(inst, held, cols, dq, dx):
        return pair(
            inst,
            dq,
            dx,
            parts.at[held, at.member(dq, dx, 1 - at.core), :, cols],
            pair_in.at[held, dq, dx, :, cols],
        )

    def sum_copy(inst, held, cols, dq, dx, direct):
        if direct:
            who = at.device(dq, dx, at.core)
        else:
            who = at.device(0, dx, at.core) if dx else at.device(dq, 0, at.core)
        return ici(
            inst,
            dq,
            dx,
            parts.at[held, at.member(dq, dx, at.core), :, cols],
            sums_in.at[held, dq, dx, :, cols],
            who,
        )

    def sum_start(inst, held, cols, direct, compute):
        def reduce_pairs(dq):
            for dx in list(range(1, xs)) + [0]:
                sum_pair(inst, held, cols, dq, dx).wait_recv()
                mine = at.member(dq, dx, at.core)
                both = parts[held, mine, :, cols].astype(F32) + pair_in[
                    held, dq, dx, :, cols
                ].astype(F32)
                if direct and dq == 0 and dx == 0:
                    total[:, cols] = both
                    continue
                parts[held, mine, :, cols] = both.astype(BF16)
                if direct or dx:
                    start(sum_copy(inst, held, cols, dq, dx, direct))

        ready = None
        for dq in list(range(1, quad)) + [0]:
            compute(at.at_q(dq))
            for dx in range(xs):
                start(sum_pair(inst, held, cols, dq, dx))
            if ready is not None:
                reduce_pairs(ready)
            ready = dq
        reduce_pairs(ready)

    def sum_pass_on(inst, held, cols):
        for dq in list(range(1, quad)) + [0]:
            mine = at.member(dq, 0, at.core)
            running = parts[held, mine, :, cols].astype(F32)
            for dx in range(1, xs):
                sum_copy(inst, held, cols, dq, dx, False).wait_recv()
                running = running + sums_in[held, dq, dx, :, cols].astype(F32)
            if dq:
                parts[held, mine, :, cols] = running.astype(BF16)
                start(sum_copy(inst, held, cols, dq, 0, False))
            else:
                total[:, cols] = running

    def sum_finish(inst, held, cols, direct):
        for dq, dx in others:
            if direct or dx == 0:
                sum_copy(inst, held, cols, dq, dx, direct).wait_recv()
                total[:, cols] += sums_in[held, dq, dx, :, cols].astype(F32)

    def by_owner(product):
        return product.astype(BF16).reshape(n_tp, tok_rows, product.shape[-1])

    def span_of(q):
        return pl.ds(pl.multiple_of(q * tile, tile), tile)

    def members_of(q):
        return pl.ds(q * n_tp, n_tp)

    def normalise(part, src):
        values = src[...].astype(F32)
        normed[part, at.me] = (values * inverse_rms(values) * pre_ref[...]).astype(BF16)

    def activations(part, q):
        tokens = normed[part, members_of(q)].reshape(tile, width)
        gate_tile = jnp.dot(tokens, all_rows(GATE), preferred_element_type=F32)
        up_tile = jnp.dot(tokens, all_rows(UP), preferred_element_type=F32)
        return gate_tile, up_tile, (gate_tile * jax.nn.sigmoid(gate_tile) * up_tile).astype(BF16)

    early_tokens, late_tokens, cot_tokens, normed_sum, late_sum, mixed_sum = range(6)

    at.enter()
    normalise(EARLY, early_ref)
    gather_start(early_tokens, normed.at[EARLY], False)
    send_weights(GATE)
    normalise(LATE, late_ref)
    gather_start(late_tokens, normed.at[LATE], False)
    send_weights(UP)
    send_weights(DOWN)
    for w in range(3):
        own = pl.ds(pl.multiple_of(at.q * units, units), units)
        weights[w, at.fs] = w_refs[w][:, own]
    gather_pass_on(early_tokens, normed.at[EARLY], False)
    gather_pass_on(late_tokens, normed.at[LATE], False)
    gather_wait(early_tokens, normed.at[EARLY])
    wait_weights(GATE, range(groups))
    wait_weights(UP, range(groups))

    @pl.loop(0, quad)
    def _(i):
        span = span_of(i)
        gate[span], up[span], hidden[span] = activations(EARLY, i)

    def chunk_of(dg):
        return pl.ds(pl.multiple_of(at.at_g(dg) * chunk, chunk), chunk)

    first_mixed = len(pending)
    for dg in range(groups):
        wait_weights(DOWN, [dg])

        def mixed_part(q, dg=dg):
            down = weights[DOWN, pl.ds(at.at_g(dg) * quad, quad)].reshape(chunk, units)
            parts[0, members_of(q), :, chunk_of(dg)] = by_owner(
                contract_last(hidden[span_of(q)], down)
            )

        sum_start(mixed_sum + dg, 0, chunk_of(dg), True, mixed_part)
    mixed_sends = pending[first_mixed:]
    del pending[first_mixed:]
    for dg in range(groups):
        sum_finish(mixed_sum + dg, 0, chunk_of(dg), True)
    mixed = total[...].astype(BF16).astype(F32)
    inverse = inverse_rms(mixed)
    weighted = 0.5 * grad_ref[...].astype(F32) * post_ref[...]
    cots[at.me] = (
        inverse * weighted
        - mixed * inverse**3 * jnp.mean(weighted * mixed, axis=-1, keepdims=True)
    ).astype(BF16)
    gather_start(cot_tokens, cots, True)
    gather_pass_on(cot_tokens, cots, True)
    gather_wait(cot_tokens, cots)

    def grad_copy(w, dg, dq):
        slot = at.slot(dg, dq)
        who = {"fs": slot, "tp": at.tp}
        return remote(
            grad_parts.at[w, slot],
            grad_in.at[w, dg, dq],
            g_send.at[w, dg, dq],
            g_recv.at[w, dg, dq],
            who,
        )

    def grad_part(w, left_ref, right_ref, dg):
        @pl.loop(0, quad)
        def _(dq):
            slot = at.slot(dg, dq)
            left = left_ref[:, :, pl.ds(pl.multiple_of(slot * rows, rows), rows)]
            left = left.reshape(quad * tile, rows)
            grad_parts[w, slot] = (grad_scale * contract_first(left, right_ref[...])).astype(BF16)

        for dq in q_order:
            if dg or dq:
                start(grad_copy(w, dg, dq))

    early_rows = normed.at[EARLY]
    for dg in range(1, groups):
        grad_part(DOWN, cots, hidden, dg)

    @pl.loop(0, quad)
    def _(i):
        span = span_of(i)
        cot = cots[members_of(i)].reshape(tile, width)
        hidden_cot = jnp.dot(cot, all_rows(DOWN), preferred_element_type=F32)
        gate_tile, up_tile = gate[span], up[span]
        sigmoid = jax.nn.sigmoid(gate_tile)
        gate_cot[span] = (
            hidden_cot * up_tile * sigmoid * (1.0 + gate_tile * (1.0 - sigmoid))
        ).astype(BF16)
        up_cot[span] = (hidden_cot * gate_tile * sigmoid).astype(BF16)

    for dg in range(1, groups):
        grad_part(GATE, early_rows, gate_cot, dg)
        grad_part(UP, early_rows, up_cot, dg)
    grad_part(DOWN, cots, hidden, 0)
    grad_part(GATE, early_rows, gate_cot, 0)
    grad_part(UP, early_rows, up_cot, 0)

    def normed_part(q):
        span = span_of(q)
        parts[1, members_of(q)] = by_owner(
            contract_last(gate_cot[span], all_rows(GATE))
            + contract_last(up_cot[span], all_rows(UP))
        )

    sum_start(normed_sum, 1, everything, False, normed_part)

    for copy in mixed_sends:
        copy.wait_send()
    gather_wait(late_tokens, normed.at[LATE])

    def late_part(q):
        parts[0, members_of(q)] = by_owner(
            contract_last(activations(LATE, q)[2], all_rows(DOWN))
        )

    sum_start(late_sum, 0, everything, False, late_part)
    sum_pass_on(normed_sum, 1, everything)
    sum_finish(normed_sum, 1, everything, False)
    values = early_ref[...].astype(F32)
    inverse = inverse_rms(values)
    weighted = total[...].astype(BF16).astype(F32) * pre_ref[...]
    early_out[...] = (
        grad_ref[...].astype(F32)
        + inverse * weighted
        - values * inverse**3 * jnp.mean(weighted * values, axis=-1, keepdims=True)
    ).astype(BF16)
    sum_pass_on(late_sum, 0, everything)
    sum_finish(late_sum, 0, everything, False)
    mixed = total[...].astype(BF16).astype(F32)
    late_out[...] = (
        late_ref[...].astype(F32) + 0.5 * mixed * inverse_rms(mixed) * post_ref[...]
    ).astype(BF16)

    for w in (DOWN, GATE, UP):
        for dq in q_order:
            running = None
            for dg in range(groups):
                if dg or dq:
                    grad_copy(w, dg, dq).wait_recv()
                    term = grad_in[w, dg, dq].astype(F32)
                else:
                    term = grad_parts[w, at.fs].astype(F32)
                running = term if running is None else running + term
            own = pl.ds(pl.multiple_of(at.at_q(-dq) * units, units), units)
            grad_outs[w][:, own] = running.astype(BF16)

    for copy in pending:
        copy.wait_send()


def per_device(
    n_fs,
    n_tp,
    late_input,
    early_input,
    early_grad,
    pre_gain,
    post_gain,
    gate_weight,
    up_weight,
    down_weight,
    gate_sum,
    up_sum,
    down_gradient_sum,
):
    tok_rows, width = late_input.shape
    rows, hidden_width = gate_weight.shape
    quad = quad_of(n_fs, n_tp)
    groups, xs, members = n_fs // quad, n_tp // PAIR, quad * n_tp
    units = hidden_width // quad
    group_rows = members * tok_rows
    grad_scale = 1.0 / math.sqrt(tok_rows * n_tp * n_fs)
    dma = pltpu.SemaphoreType.DMA
    operands = (
        late_input,
        early_input,
        early_grad,
        pre_gain.reshape(1, width),
        post_gain.reshape(1, width),
        gate_weight,
        up_weight,
        down_weight,
    )
    outs = [jax.ShapeDtypeStruct((tok_rows, width), BF16)] * 2 + [
        jax.ShapeDtypeStruct((rows, hidden_width), BF16)
    ] * 3
    in_vmem = pl.BlockSpec(memory_space=pltpu.VMEM)
    late_output, early_input_grad, *grads = pl.pallas_call(
        functools.partial(layer_kernel, n_fs, n_tp, grad_scale),
        out_shape=outs,
        in_specs=[in_vmem] * len(operands),
        out_specs=[in_vmem] * len(outs),
        scratch_shapes=[
            pltpu.VMEM((2, members, tok_rows, width), BF16),
            pltpu.VMEM((3, n_fs, rows, units), BF16),
            pltpu.VMEM((group_rows, units), F32),
            pltpu.VMEM((group_rows, units), F32),
            pltpu.VMEM((group_rows, units), BF16),
            pltpu.VMEM((members, tok_rows, width), BF16),
            pltpu.VMEM((2, members, tok_rows, width), BF16),
            pltpu.VMEM((2, quad, xs, tok_rows, width), BF16),
            pltpu.VMEM((2, quad, xs, tok_rows, width), BF16),
            pltpu.VMEM((tok_rows, width), F32),
            pltpu.VMEM((group_rows, units), BF16),
            pltpu.VMEM((group_rows, units), BF16),
            pltpu.VMEM((3, n_fs, rows, units), BF16),
            pltpu.VMEM((3, groups, quad, rows, units), BF16),
        ]
        + [dma((3, groups, quad))] * 4
        + [dma((5 + groups, 4, quad, xs))],
        cost_estimate=pl.CostEstimate(flops=10**9, bytes_accessed=0, transcendentals=0),
        compiler_params=pltpu.CompilerParams(
            collective_id=0, has_side_effects=True, vmem_limit_bytes=VMEM_LIMIT
        ),
    )(*operands)
    totals = [
        running + grad.astype(F32)
        for running, grad in zip((gate_sum, up_sum, down_gradient_sum), grads)
    ]
    return (late_output, early_input_grad, *totals)


def solution(mesh):
    in_specs = (
        P(("fs", "tp"), None),
        P(("fs", "tp"), None),
        P(("fs", "tp"), None),
        P(),
        P(),
        P("fs", "tp"),
        P("fs", "tp"),
        P("fs", "tp"),
        P("fs", "tp"),
        P("fs", "tp"),
        P("fs", "tp"),
    )
    out_specs = (
        P(("fs", "tp"), None),
        P(("fs", "tp"), None),
        P("fs", "tp"),
        P("fs", "tp"),
        P("fs", "tp"),
    )
    return jax.shard_map(
        functools.partial(per_device, mesh.shape["fs"], mesh.shape["tp"]),
        mesh=mesh, in_specs=in_specs, out_specs=out_specs, check_vma=False
    )
```

time: 286 us -> 238 us (0.83)
  the two profiles are of different devices: /device:TPU:0 before, /device:TPU:7 now
where the time goes in v1:
time: 238 us
  Pallas kernels  231 us (97%)
  other arithmetic  4.19 us (2%)
    pallas_call x1, Pallas kernels, per_device(): pl.pallas_call(functools.partial(layer_kernel, n_fs, n_tp, grad_scale), o...  231 us

profile of v1, /device:TPU:7, one launch (start us, length us, event | category | flops | bytes accessed | tf_op | source)
XLA Modules:
  0.0 237.5 jit_solution(1279933600816501567)
XLA Ops:
  0.6 0.0 copy-start
  0.6 0.0 copy-start.1
  0.7 230.9 %shard_map.146 = (bf16[64,2048]{1,0:T(8,128)(2,1)}, bf16[64,2048]{1,0:T(8,128)(2,1)}, bf16[256,1024]{1,0:T(8,128)(2,1)}, bf16[256,1024]{1,0:T(8,128)(2,1)}, bf16[256,1024]{1,0:T(8,128)(2,1)}) custom-call(bf16[64,2048]{1,0:T(8,128)(2,1)} %refs_0_.1, bf16[64,2048]{1,0:T(8,128)(2,1)} %refs_1_.1, bf16[64,2048]{1,0:T(8,128)(2,1)} %refs_2_.1, f32[1,2048]{1,0:T(1,128)} %bitcast.2, ...), custom_call_target="tpu_custom_call" | custom-call | flops 1000000000 | tf_op jit(solution)/shard_map/pallas_call | solution.py:462
  231.5 0.0 copy-done
  231.6 0.0 copy-done.1
  231.6 0.0 copy-start.2
  231.6 0.0 copy-start.3
  231.6 3.1 %convert_add_fusion = (f32[256,1024]{1,0:T(8,128)}, f32[256,1024]{1,0:T(8,128)}) fusion(f32[256,1024]{1,0:T(8,128)S(1)} %copy-done, bf16[256,1024]{1,0:T(8,128)(2,1)} %get-tuple-element.14, f32[256,1024]{1,0:T(8,128)S(1)} %copy-done.1, bf16[256,1024]{1,0:T(8,128)(2,1)} %get-tuple-element.13), kind=kLoop, calls=%fused_computation | loop fusion | flops 1048576 | bytes 5242880 | tf_op jit(solution)/shard_map/add | solution.py:491
  234.7 0.0 copy-done.2
  234.7 0.0 copy-done.3
  234.7 0.0 copy-start.5
  234.7 1.1 convert_add_fusion.2
  235.8 0.0 copy-done.5
  235.8 0.0 copy-start.4
  235.8 0.7 copy.18
  236.5 0.3 copy-done.4
  236.8 0.7 copy.19
Async XLA Ops:
  0.6 230.9 %copy-start = (f32[256,1024]{1,0:T(8,128)S(1)}, f32[256,1024]{1,0:T(8,128)}, u32[]{:S(2)}) copy-start(f32[256,1024]{1,0:T(8,128)} %param.21) | copy-start | bytes 3145732
  0.6 230.9 %copy-start.1 = (f32[256,1024]{1,0:T(8,128)S(1)}, f32[256,1024]{1,0:T(8,128)}, u32[]{:S(2)}) copy-start(f32[256,1024]{1,0:T(8,128)} %param.20) | copy-start | bytes 3145732
  231.6 3.1 %copy-start.2 = (f32[256,1024]{1,0:T(8,128)S(1)}, f32[256,1024]{1,0:T(8,128)}, u32[]{:S(2)}) copy-start(f32[256,1024]{1,0:T(8,128)} %param.19) | copy-start | bytes 3145732
  231.6 3.1 %copy-start.3 = (bf16[256,1024]{1,0:T(8,128)(2,1)S(1)}, bf16[256,1024]{1,0:T(8,128)(2,1)}, u32[]{:S(2)}) copy-start(bf16[256,1024]{1,0:T(8,128)(2,1)} %get-tuple-element.12) | copy-start | bytes 1572868
  234.7 1.1 copy-start.5
  235.8 1.0 copy-start.4

commit v2 on v1

v2 whole, which is shorter than its diff:
```python
import functools
import math

import jax
import jax.numpy as jnp
from jax import lax
from jax.experimental import pallas as pl
from jax.experimental.pallas import tpu as pltpu
from jax.sharding import PartitionSpec as P

NORM_EPS = 1e-06
PAIR = 2
GROUP = 16
LATE, EARLY = 0, 1
GATE, UP, DOWN = 0, 1, 2
MESH = pl.DeviceIdType.MESH
VMEM_LIMIT = 48 * 1024 * 1024
LANES = 128
BF16, F32 = jnp.bfloat16, jnp.float32
scope = jax.named_scope
LAST_PHASE = (
    "late_send", "down_far", "down_far_crossing", "down_near", "down_near_crossing",
    "down_far_straight", "hidden_cots", "gate_far", "gate_far_crossing", "gate_near",
    "gate_near_crossing", "up_far", "gate_far_straight", "up_far_straight", "normed_start",
    "up_near", "down_near_straight", "gate_near_straight", "late_1", "up_near_crossing",
    "late_2", "normed_1", "up_far_crossing", "up_near_straight", "normed_2", "late_end",
    "normed_end",
)


def contract_last(first_op, second_op):
    return lax.dot_general(
        first_op, second_op, (((1,), (1,)), ((), ())), preferred_element_type=F32
    )


def contract_first(first_op, second_op):
    return lax.dot_general(
        first_op, second_op, (((0,), (0,)), ((), ())), preferred_element_type=F32
    )


def inverse_rms(values):
    return lax.rsqrt(jnp.mean(values * values, axis=-1, keepdims=True) + NORM_EPS)


def quad_of(n_fs, n_tp):
    return min(n_fs, max(1, GROUP // n_tp))


def shape_of(n_fs, n_tp):
    quad = quad_of(n_fs, n_tp)
    deep = PAIR if quad % PAIR == 0 else 1
    return quad // deep, deep, n_tp // PAIR


class Place:
    def __init__(self, n_fs, n_tp):
        self.n_fs, self.n_tp = n_fs, n_tp
        self.quad = quad_of(n_fs, n_tp)
        self.groups = n_fs // self.quad
        self.sizes = shape_of(n_fs, n_tp)
        self.fs, self.tp = lax.axis_index("fs"), lax.axis_index("tp")
        self.g, self.q = self.fs // self.quad, self.fs % self.quad
        self.core = self.tp % PAIR
        self.coords = (self.q // self.sizes[1], self.q % self.sizes[1], self.tp // PAIR)
        self.offsets = [
            (i, j, k)
            for i in range(self.sizes[0])
            for j in range(self.sizes[1])
            for k in range(self.sizes[2])
        ]
        self.me = self.member((0, 0, 0), 1, self.core)
        self.partner = self.device((0, 0, 0), 1 - self.core)

    def moved(self, offset, sign):
        return [
            (c + size + sign * o) % size
            for c, size, o in zip(self.coords, self.sizes, offset)
        ]

    def member(self, offset, sign, core):
        i, j, k = self.moved(offset, sign)
        return (i * self.sizes[1] + j) * self.n_tp + k * PAIR + core

    def device(self, offset, core):
        i, j, k = self.moved(offset, 1)
        return {"fs": self.g * self.quad + i * self.sizes[1] + j, "tp": k * PAIR + core}

    def flat(self, offset):
        return (offset[0] * self.sizes[1] + offset[1]) * self.sizes[2] + offset[2]

    def at_q(self, dq):
        return (self.q + self.quad + dq) % self.quad

    def at_g(self, dg):
        return (self.g + dg) % self.groups

    def slot(self, dg, dq):
        return self.at_g(dg) * self.quad + self.at_q(dq)

    def enter(self):
        barrier = pltpu.get_barrier_semaphore()

        def greet(fs, tp):
            pl.semaphore_signal(
                barrier, inc=1, device_id={"fs": fs, "tp": tp}, device_id_type=MESH
            )

        peers = 0
        for offset in range(1, self.n_fs):
            greet((self.fs + offset) % self.n_fs, self.tp)
            peers += 1
        for dq in range(self.quad):
            for offset in range(1, self.n_tp):
                greet(self.g * self.quad + self.at_q(dq), (self.tp + offset) % self.n_tp)
                peers += 1
        pl.semaphore_wait(barrier, peers)


def remote(src, dst, send_sem, recv_sem, who):
    return pltpu.make_async_remote_copy(
        src_ref=src,
        dst_ref=dst,
        send_sem=send_sem,
        recv_sem=recv_sem,
        device_id=who,
        device_id_type=MESH,
    )


def layer_kernel(n_fs, n_tp, grad_scale, *refs):
    sources = refs[:8]
    late_out, early_out = refs[8:10]
    grad_outs = refs[10:13]
    normed, weights, gate, up, hidden, cots, parts, pair_in, sums_in, total = refs[13:23]
    gate_cot, up_cot, grad_parts, grad_in, hidden_late = refs[23:28]
    late_ref, early_ref, grad_ref, pre_ref, post_ref = refs[28:33]
    w_refs = refs[33:36]
    w_send, w_recv, g_send, g_recv, sems, load_sem = refs[36:]
    loads = [
        pltpu.make_async_copy(src, dst, load_sem.at[i])
        for i, (src, dst) in enumerate(zip(sources, refs[28:36]))
    ]
    for i in (1, 3, 5, 0, 6, 7, 2, 4):
        loads[i].start()

    at = Place(n_fs, n_tp)
    quad, groups, sizes, offsets = at.quad, at.groups, at.sizes, at.offsets
    home, others = offsets[0], offsets[1:]
    tok_rows, width = early_ref.shape
    rows, units = weights.shape[2:]
    tile = n_tp * tok_rows
    chunk = quad * rows
    pending = []

    def start(copy):
        copy.start()
        pending.append(copy)

    def w_copy(w, dg, dq):
        source = w_refs[w].at[:, pl.ds(pl.multiple_of(at.at_q(dq) * units, units), units)]
        who = {"fs": at.slot(dg, dq), "tp": at.tp}
        return remote(
            source, weights.at[w, at.fs], w_send.at[w, dg, dq], w_recv.at[w, dg, dq], who
        )

    q_order = [1, 3, 2, 0] if quad == 4 else list(range(quad - 1, -1, -1))

    def send_weights(w):
        for dq in q_order:
            for dg in range(groups - 1, -1, -1):
                if dg or dq:
                    start(w_copy(w, dg, dq))

    def wait_weights(w, dgs):
        for dg in dgs:
            for dq in q_order:
                if dg or dq:
                    w_copy(w, dg, dq).wait_recv()

    def all_rows(w):
        return weights[w].reshape(n_fs * rows, units)

    def place_in(order, offset, last):
        found = [p for p, axis in enumerate(order) if offset[axis]]
        if not found:
            return -1 if last else len(order)
        return found[-1] if last else found[0]

    def put(offset, axis, value):
        return tuple(value if i == axis else o for i, o in enumerate(offset))

    def along(offset, axis):
        return tuple(o if i == axis else 0 for i, o in enumerate(offset))

    def steps(axis):
        return range(1, sizes[axis])

    def hops(offset):
        return sum(1 for o in offset if o)

    def cols_of(route):
        return pl.ds(route[2], route[3])

    def ici(inst, offset, src, dst, who):
        i = at.flat(offset)
        return remote(src, dst, sems.at[inst, 0, i], sems.at[inst, 1, i], who)

    def pair(inst, offset, src, dst):
        i = at.flat(offset)
        return remote(src, dst, sems.at[inst, 2, i], sems.at[inst, 3, i], at.partner)

    def gather_copy(buf, route, offset):
        axis = route[1][place_in(route[1], offset, True)]
        block = buf.at[at.member(put(offset, axis, 0), -1, at.core), :, cols_of(route)]
        return ici(route[0], offset, block, block, at.device(along(offset, axis), at.core))

    def gather_pair(buf, route, offset):
        block = buf.at[at.member(offset, -1, at.core), :, cols_of(route)]
        return pair(route[0], offset, block, block)

    def onward(route, offset):
        order = route[1]
        later = order[place_in(order, offset, True) + 1 :]
        return [put(offset, axis, e) for axis in later for e in steps(axis)]

    def gather_start(buf, routes):
        sends = [(route, offset) for route in routes for offset in onward(route, home)]
        sends.sort(key=lambda send: place_in(send[0][1], send[1], True))
        for route, offset in sends:
            start(gather_copy(buf, route, offset))
        for route in routes:
            start(gather_pair(buf, route, home))

    def gather_pass_on(buf, routes, stages=range(3)):
        arrivals = [(route, offset) for route in routes for offset in others]
        arrivals = [a for a in arrivals if place_in(a[0][1], a[1], True) in stages]
        arrivals.sort(key=lambda a: (hops(a[1]), place_in(a[0][1], a[1], True)))
        for route, offset in arrivals:
            gather_copy(buf, route, offset).wait_recv()
            for further in onward(route, offset):
                start(gather_copy(buf, route, further))
            start(gather_pair(buf, route, offset))

    def gather_wait(buf, routes):
        for route in routes:
            for offset in offsets:
                gather_pair(buf, route, offset).wait_recv()

    def sum_pair(held, routes, offset):
        cols = pl.ds(routes[0][2], sum(route[3] for route in routes))
        return pair(
            routes[0][0],
            offset,
            parts.at[held, at.member(offset, 1, 1 - at.core), :, cols],
            pair_in.at[held, at.flat(offset), :, cols],
        )

    def sum_copy(held, route, offset):
        axis = route[1][place_in(route[1], offset, False)]
        return ici(
            route[0],
            offset,
            parts.at[held, at.member(offset, 1, at.core), :, cols_of(route)],
            sums_in.at[held, at.flat(offset), :, cols_of(route)],
            at.device(along(offset, axis), at.core),
        )

    def sum_block(held, route, offset):
        cols, mine = cols_of(route), at.member(offset, 1, at.core)
        running = parts[held, mine, :, cols].astype(F32)
        running = running + pair_in[held, at.flat(offset), :, cols].astype(F32)
        for axis in route[1][: place_in(route[1], offset, False)]:
            for e in steps(axis):
                came = put(offset, axis, e)
                sum_copy(held, route, came).wait_recv()
                running = running + sums_in[held, at.flat(came), :, cols].astype(F32)
        if offset == home:
            total[:, cols] = running
        else:
            parts[held, mine, :, cols] = running.astype(BF16)
            start(sum_copy(held, route, offset))

    def sum_send(held, routes, ready):
        for offset in ready:
            sum_pair(held, routes, offset).wait_recv()
        for route in routes:
            for offset in ready:
                if place_in(route[1], offset, False) == 0:
                    sum_block(held, route, offset)

    def sum_start(held, routes, compute, send=True):
        ready = []
        for pos in sorted({offset[:2] for offset in offsets}, key=lambda p: (-hops(p), p)):
            now = sorted((o for o in offsets if o[:2] == pos), key=hops, reverse=True)
            i, j, _ = at.moved(now[0], 1)
            compute(i * sizes[1] + j)
            for offset in now:
                start(sum_pair(held, routes, offset))
            if send:
                sum_send(held, routes, ready)
            ready = now
        if send:
            sum_send(held, routes, ready)

    def sum_finish(held, routes, stages=(1, 2, 3)):
        rest = [(route, offset) for route in routes for offset in offsets]
        rest = [r for r in rest if place_in(r[0][1], r[1], False) in stages]
        rest.sort(key=lambda r: (place_in(r[0][1], r[1], False), -hops(r[1])))
        for route, offset in rest:
            sum_block(held, route, offset)

    def by_owner(product):
        return product.astype(BF16).reshape(n_tp, tok_rows, product.shape[-1])

    def span_of(q):
        return pl.ds(pl.multiple_of(q * tile, tile), tile)

    def members_of(q):
        return pl.ds(q * n_tp, n_tp)

    def normalise(part, src):
        values = src[...].astype(F32)
        normed[part, at.me] = (values * inverse_rms(values) * pre_ref[...]).astype(BF16)

    def activations(part, q):
        tokens = normed[part, members_of(q)].reshape(tile, width)
        gate_tile = jnp.dot(tokens, all_rows(GATE), preferred_element_type=F32)
        up_tile = jnp.dot(tokens, all_rows(UP), preferred_element_type=F32)
        return gate_tile, up_tile, (gate_tile * jax.nn.sigmoid(gate_tile) * up_tile).astype(BF16)

    z, y, x = range(3)
    early_tokens, late_tokens = [(0, (z, y, x), 0, width)], [(1, (z, y, x), 0, width)]
    normed_sum, late_sum = [(2, (x, y, z), 0, width)], [(3, (x, y, z), 0, width)]

    def balanced(first, begin, size):
        routes, done = [], 0
        for i, order in enumerate(((x, y, z), (y, z, x), (z, x, y))):
            end = (i + 1) * (size // LANES) // 3 * LANES
            if end > done:
                col = begin + done
                col = col if isinstance(col, int) else pl.multiple_of(col, LANES)
                routes.append((first + i, order, col, end - done))
            done = end
        return routes

    cot_tokens = balanced(4, 0, width)

    def mixed_sum(dg):
        return balanced(7 + 3 * dg, at.at_g(dg) * chunk, chunk)

    with scope("enter"):
        at.enter()
    early_buf, late_buf = normed.at[EARLY], normed.at[LATE]
    with scope("issue"):
        for load in loads:
            load.wait()
        normalise(EARLY, early_ref)
        gather_start(early_buf, early_tokens)
        send_weights(GATE)
        normalise(LATE, late_ref)
        gather_start(late_buf, late_tokens)
        for w in range(3):
            own = pl.ds(pl.multiple_of(at.q * units, units), units)
            weights[w, at.fs] = w_refs[w][:, own]
    with scope("early_stage_0"):
        gather_pass_on(early_buf, early_tokens, [0])
        send_weights(UP)
    with scope("early_stage_1"):
        gather_pass_on(early_buf, early_tokens, [1])
    with scope("late_stage_0"):
        gather_pass_on(late_buf, late_tokens, [0])
        send_weights(DOWN)
    with scope("early_stage_2"):
        gather_pass_on(early_buf, early_tokens, [2])
    with scope("late_stage_1"):
        gather_pass_on(late_buf, late_tokens, [1])
    with scope("early_wait"):
        gather_wait(early_buf, early_tokens)
    with scope("gate_wait"):
        wait_weights(GATE, range(groups))
    with scope("up_wait"):
        wait_weights(UP, range(groups))

    with scope("early_forward"):

        @pl.loop(0, quad)
        def _(i):
            span = span_of(i)
            gate[span], up[span], hidden[span] = activations(EARLY, i)

    with scope("late_stage_2"):
        gather_pass_on(late_buf, late_tokens, [2])
        gather_wait(late_buf, late_tokens)
    with scope("late_hidden"):

        @pl.loop(0, quad)
        def _(i):
            hidden_late[span_of(i)] = activations(LATE, i)[2]

    def chunk_of(dg):
        return pl.ds(pl.multiple_of(at.at_g(dg) * chunk, chunk), chunk)

    first_mixed = len(pending)
    for dg in range(groups):
        with scope(f"down_wait_{dg}"):
            wait_weights(DOWN, [dg])

        def mixed_part(q, dg=dg):
            down = weights[DOWN, pl.ds(at.at_g(dg) * quad, quad)].reshape(chunk, units)
            parts[0, members_of(q), :, chunk_of(dg)] = by_owner(
                contract_last(hidden[span_of(q)], down)
            )

        with scope(f"mixed_{dg}"):
            sum_start(0, mixed_sum(dg), mixed_part)
    for stage in (1, 2, 3):
        with scope(f"mixed_finish_{stage}"):
            for dg in range(groups):
                sum_finish(0, mixed_sum(dg), [stage])
    mixed_sends = pending[first_mixed:]
    del pending[first_mixed:]
    with scope("mixed_cot"):
        mixed = total[...].astype(BF16).astype(F32)
        inverse = inverse_rms(mixed)
        weighted = 0.5 * grad_ref[...].astype(F32) * post_ref[...]
        cots[at.me] = (
            inverse * weighted
            - mixed * inverse**3 * jnp.mean(weighted * mixed, axis=-1, keepdims=True)
        ).astype(BF16)
        gather_start(cots, cot_tokens)

    def late_part(q):
        parts[1, members_of(q)] = by_owner(contract_last(hidden_late[span_of(q)], all_rows(DOWN)))

    with scope("late_sum"):
        sum_start(1, late_sum, late_part, send=False)
    with scope("cot_tokens"):
        gather_pass_on(cots, cot_tokens)
        gather_wait(cots, cot_tokens)

    def grad_copy(w, dg, dq):
        slot = at.slot(dg, dq)
        who = {"fs": slot, "tp": at.tp}
        return remote(
            grad_parts.at[w, slot],
            grad_in.at[w, dg, dq],
            g_send.at[w, dg, dq],
            g_recv.at[w, dg, dq],
            who,
        )

    def grad_part(w, left_ref, right_ref, dg):
        @pl.loop(0, quad)
        def _(dq):
            slot = at.slot(dg, dq)
            left = left_ref[:, :, pl.ds(pl.multiple_of(slot * rows, rows), rows)]
            left = left.reshape(quad * tile, rows)
            grad_parts[w, slot] = (grad_scale * contract_first(left, right_ref[...])).astype(BF16)

    far = range(1, groups)
    straight = [dq for dq in q_order if dq % sizes[1] == 0]
    crossing = [dq for dq in q_order if dq % sizes[1]]

    def send_grads(w, dgs, dqs):
        for dq in dqs:
            for dg in dgs:
                if dg or dq:
                    start(grad_copy(w, dg, dq))

    early_rows = normed.at[EARLY]
    def hidden_cots():
        @pl.loop(0, quad)
        def _(i):
            span = span_of(i)
            cot = cots[members_of(i)].reshape(tile, width)
            hidden_cot = jnp.dot(cot, all_rows(DOWN), preferred_element_type=F32)
            gate_tile, up_tile = gate[span], up[span]
            sigmoid = jax.nn.sigmoid(gate_tile)
            gate_cot[span] = (
                hidden_cot * up_tile * sigmoid * (1.0 + gate_tile * (1.0 - sigmoid))
            ).astype(BF16)
            up_cot[span] = (hidden_cot * gate_tile * sigmoid).astype(BF16)

    def normed_part(q):
        span = span_of(q)
        parts[0, members_of(q)] = by_owner(
            contract_last(gate_cot[span], all_rows(GATE))
            + contract_last(up_cot[span], all_rows(UP))
        )

    def normed_start():
        for copy in mixed_sends:
            copy.wait_send()
        sum_start(0, normed_sum, normed_part)

    def late_end():
        sum_finish(1, late_sum, [3])
        mixed = total[...].astype(BF16).astype(F32)
        late_out[...] = (
            late_ref[...].astype(F32) + 0.5 * mixed * inverse_rms(mixed) * post_ref[...]
        ).astype(BF16)

    def normed_end():
        sum_finish(0, normed_sum, [3])
        values = early_ref[...].astype(F32)
        inverse = inverse_rms(values)
        weighted = total[...].astype(BF16).astype(F32) * pre_ref[...]
        early_out[...] = (
            grad_ref[...].astype(F32)
            + inverse * weighted
            - values * inverse**3 * jnp.mean(weighted * values, axis=-1, keepdims=True)
        ).astype(BF16)

    operands_of = {DOWN: (cots, hidden), GATE: (early_rows, gate_cot), UP: (early_rows, up_cot)}

    def compute_grads(w, dgs):
        for dg in dgs:
            grad_part(w, *operands_of[w], dg)

    steps_by_name = {
        "late_send": lambda: sum_send(1, late_sum, offsets),
        "hidden_cots": hidden_cots,
        "normed_start": normed_start,
        "late_1": lambda: sum_finish(1, late_sum, [1]),
        "late_2": lambda: sum_finish(1, late_sum, [2]),
        "late_end": late_end,
        "normed_1": lambda: sum_finish(0, normed_sum, [1]),
        "normed_2": lambda: sum_finish(0, normed_sum, [2]),
        "normed_end": normed_end,
    }
    for name, w in (("down", DOWN), ("gate", GATE), ("up", UP)):
        for where, dgs in (("far", far), ("near", [0])):
            steps_by_name[f"{name}_{where}"] = functools.partial(compute_grads, w, dgs)
            for way, dqs in (("straight", straight), ("crossing", crossing)):
                steps_by_name[f"{name}_{where}_{way}"] = functools.partial(
                    send_grads, w, dgs, dqs
                )
    for name in LAST_PHASE:
        with scope(name):
            steps_by_name[name]()

    for w in (DOWN, GATE, UP):
        with scope(f"grad_out_{w}"):
            for dq in q_order:
                running = None
                for dg in range(groups):
                    if dg or dq:
                        grad_copy(w, dg, dq).wait_recv()
                        term = grad_in[w, dg, dq].astype(F32)
                    else:
                        term = grad_parts[w, at.fs].astype(F32)
                    running = term if running is None else running + term
                own = pl.ds(pl.multiple_of(at.at_q(-dq) * units, units), units)
                grad_outs[w][:, own] = running.astype(BF16)

    with scope("drain"):
        for copy in pending:
            copy.wait_send()


def per_device(
    n_fs,
    n_tp,
    late_input,
    early_input,
    early_grad,
    pre_gain,
    post_gain,
    gate_weight,
    up_weight,
    down_weight,
    gate_sum,
    up_sum,
    down_gradient_sum,
):
    tok_rows, width = late_input.shape
    rows, hidden_width = gate_weight.shape
    quad = quad_of(n_fs, n_tp)
    groups, members = n_fs // quad, quad * n_tp
    units = hidden_width // quad
    group_rows = members * tok_rows
    grad_scale = 1.0 / math.sqrt(tok_rows * n_tp * n_fs)
    dma = pltpu.SemaphoreType.DMA
    operands = (
        late_input,
        early_input,
        early_grad,
        pre_gain.reshape(1, width),
        post_gain.reshape(1, width),
        gate_weight,
        up_weight,
        down_weight,
    )
    outs = [jax.ShapeDtypeStruct((tok_rows, width), BF16)] * 2 + [
        jax.ShapeDtypeStruct((rows, hidden_width), BF16)
    ] * 3
    in_vmem = pl.BlockSpec(memory_space=pltpu.VMEM)
    late_output, early_input_grad, *grads = pl.pallas_call(
        functools.partial(layer_kernel, n_fs, n_tp, grad_scale),
        out_shape=outs,
        in_specs=[pl.BlockSpec(memory_space=pltpu.HBM)] * len(operands),
        out_specs=[in_vmem] * len(outs),
        scratch_shapes=[
            pltpu.VMEM((2, members, tok_rows, width), BF16),
            pltpu.VMEM((3, n_fs, rows, units), BF16),
            pltpu.VMEM((group_rows, units), F32),
            pltpu.VMEM((group_rows, units), F32),
            pltpu.VMEM((group_rows, units), BF16),
            pltpu.VMEM((members, tok_rows, width), BF16),
            pltpu.VMEM((2, members, tok_rows, width), BF16),
            pltpu.VMEM((2, members // PAIR, tok_rows, width), BF16),
            pltpu.VMEM((2, members // PAIR, tok_rows, width), BF16),
            pltpu.VMEM((tok_rows, width), F32),
            pltpu.VMEM((group_rows, units), BF16),
            pltpu.VMEM((group_rows, units), BF16),
            pltpu.VMEM((3, n_fs, rows, units), BF16),
            pltpu.VMEM((3, groups, quad, rows, units), BF16),
            pltpu.VMEM((group_rows, units), BF16),
        ]
        + [pltpu.VMEM(array.shape, array.dtype) for array in operands]
        + [dma((3, groups, quad))] * 4
        + [dma((7 + 3 * groups, 4, members // PAIR)), dma((len(operands),))],
        cost_estimate=pl.CostEstimate(flops=10**9, bytes_accessed=0, transcendentals=0),
        compiler_params=pltpu.CompilerParams(
            collective_id=0, has_side_effects=True, vmem_limit_bytes=VMEM_LIMIT
        ),
    )(*[pltpu.with_memory_space_constraint(array, pltpu.HBM) for array in operands])
    totals = [
        running + grad.astype(F32)
        for running, grad in zip((gate_sum, up_sum, down_gradient_sum), grads)
    ]
    return (late_output, early_input_grad, *totals)


def solution(mesh):
    in_specs = (
        P(("fs", "tp"), None),
        P(("fs", "tp"), None),
        P(("fs", "tp"), None),
        P(),
        P(),
        P("fs", "tp"),
        P("fs", "tp"),
        P("fs", "tp"),
        P("fs", "tp"),
        P("fs", "tp"),
        P("fs", "tp"),
    )
    out_specs = (
        P(("fs", "tp"), None),
        P(("fs", "tp"), None),
        P("fs", "tp"),
        P("fs", "tp"),
        P("fs", "tp"),
    )
    return jax.shard_map(
        functools.partial(per_device, mesh.shape["fs"], mesh.shape["tp"]),
        mesh=mesh, in_specs=in_specs, out_specs=out_specs, check_vma=False
    )
```

time: 238 us -> 191 us (0.80)
  the two profiles are of different devices: /device:TPU:7 before, /device:TPU:0 now
where the time goes in v2:
time: 191 us; the launch traced here: 190 us
  Pallas kernels  185 us (97%)
  other arithmetic  2.89 us (2%)
    pallas_call x1, Pallas kernels, per_device(): pl.pallas_call(functools.partial(layer_kernel, n_fs, n_tp, grad_scale), o...  185 us

profile of v2, /device:TPU:0, one launch (start us, length us, event | category | flops | bytes accessed | tf_op | source)
XLA Modules:
  0.0 189.8 jit_solution(16238744260171361187)
XLA Ops:
  0.6 0.0 copy-start
  0.6 0.0 copy-start.1
  0.7 184.8 %shard_map.146 = (bf16[64,2048]{1,0:T(8,128)(2,1)S(1)}, bf16[64,2048]{1,0:T(8,128)(2,1)S(1)}, bf16[256,1024]{1,0:T(8,128)(2,1)S(1)}, bf16[256,1024]{1,0:T(8,128)(2,1)S(1)}, bf16[256,1024]{1,0:T(8,128)(2,1)S(1)}) custom-call(bf16[64,2048]{1,0:T(8,128)(2,1)} %refs_0_.1, bf16[64,2048]{1,0:T(8,128)(2,1)} %refs_1_.1, bf16[64,2048]{1,0:T(8,128)(2,1)} %refs_2_.1, ...), custom_call_target="tpu_custom_call" | custom-call | flops 1000000000 | tf_op jit(solution)/shard_map/pallas_call | solution.py:600
  185.4 0.0 copy-done
  185.4 0.0 copy-done.1
  185.5 0.0 copy-start.2
  185.5 1.8 convert_add_fusion
  187.2 0.0 copy-done.2
  187.2 1.1 convert_add_fusion.2
  188.4 0.7 copy.18
  189.1 0.7 copy.19
Async XLA Ops:
  0.6 184.8 %copy-start = (f32[256,1024]{1,0:T(8,128)S(1)}, f32[256,1024]{1,0:T(8,128)}, u32[]{:S(2)}) copy-start(f32[256,1024]{1,0:T(8,128)} %param.21) | copy-start | bytes 3145732
  0.6 184.8 %copy-start.1 = (f32[256,1024]{1,0:T(8,128)S(1)}, f32[256,1024]{1,0:T(8,128)}, u32[]{:S(2)}) copy-start(f32[256,1024]{1,0:T(8,128)} %param.20) | copy-start | bytes 3145732
  185.5 1.8 copy-start.2

commit v3 on v2

--- a/solution.py
+++ b/solution.py
@@ -14,17 +14,17 @@
 LATE, EARLY = 0, 1
 GATE, UP, DOWN = 0, 1, 2
 MESH = pl.DeviceIdType.MESH
-VMEM_LIMIT = 48 * 1024 * 1024
+VMEM_LIMIT = 46 * 1024 * 1024
 LANES = 128
 BF16, F32 = jnp.bfloat16, jnp.float32
 scope = jax.named_scope
 LAST_PHASE = (
-    "late_send", "down_far", "down_far_crossing", "down_near", "down_near_crossing",
+    "down_far", "down_far_crossing", "late_send", "down_near", "down_near_crossing",
     "down_far_straight", "hidden_cots", "gate_far", "gate_far_crossing", "gate_near",
-    "gate_near_crossing", "up_far", "gate_far_straight", "up_far_straight", "normed_start",
-    "up_near", "down_near_straight", "gate_near_straight", "late_1", "up_near_crossing",
-    "late_2", "normed_1", "up_far_crossing", "up_near_straight", "normed_2", "late_end",
-    "normed_end",
+    "gate_near_crossing", "up_far", "gate_far_straight", "normed_start", "up_near", "late_1",
+    "up_far_straight", "down_near_straight", "up_near_crossing", "late_2",
+    "gate_near_straight", "normed_1", "up_far_crossing", "up_near_straight", "normed_2",
+    "late_end", "normed_end",
 )
 
 

time: 191 us -> 190 us (level)
  no operation moved by 1% of the time
where the time goes in v3:
time: 190 us
  Pallas kernels  185 us (97%)
  other arithmetic  2.89 us (2%)
    pallas_call x1, Pallas kernels, per_device(): pl.pallas_call(functools.partial(layer_kernel, n_fs, n_tp, grad_scale), o...  185 us

profile of v3, /device:TPU:0, one launch (start us, length us, event | category | flops | bytes accessed | tf_op | source)
XLA Modules:
  0.0 189.6 jit_solution(278109512252374762)
XLA Ops:
  0.6 0.0 copy-start
  0.6 0.0 copy-start.1
  0.7 184.6 %shard_map.146 = (bf16[64,2048]{1,0:T(8,128)(2,1)S(1)}, bf16[64,2048]{1,0:T(8,128)(2,1)S(1)}, bf16[256,1024]{1,0:T(8,128)(2,1)S(1)}, bf16[256,1024]{1,0:T(8,128)(2,1)S(1)}, bf16[256,1024]{1,0:T(8,128)(2,1)S(1)}) custom-call(bf16[64,2048]{1,0:T(8,128)(2,1)} %refs_0_.1, bf16[64,2048]{1,0:T(8,128)(2,1)} %refs_1_.1, bf16[64,2048]{1,0:T(8,128)(2,1)} %refs_2_.1, ...), custom_call_target="tpu_custom_call" | custom-call | flops 1000000000 | tf_op jit(solution)/shard_map/pallas_call | solution.py:600
  185.3 0.0 copy-done
  185.3 0.0 copy-done.1
  185.3 0.0 copy-start.2
  185.3 1.8 convert_add_fusion
  187.1 0.0 copy-done.2
  187.1 1.1 convert_add_fusion.2
  188.2 0.7 copy.18
  188.9 0.7 copy.19
Async XLA Ops:
  0.6 184.7 %copy-start = (f32[256,1024]{1,0:T(8,128)S(1)}, f32[256,1024]{1,0:T(8,128)}, u32[]{:S(2)}) copy-start(f32[256,1024]{1,0:T(8,128)} %param.21) | copy-start | bytes 3145732
  0.6 184.7 %copy-start.1 = (f32[256,1024]{1,0:T(8,128)S(1)}, f32[256,1024]{1,0:T(8,128)}, u32[]{:S(2)}) copy-start(f32[256,1024]{1,0:T(8,128)} %param.20) | copy-start | bytes 3145732
  185.3 1.8 copy-start.2
